TPU v7x, 32 devices: a whole 2x2x4 slice. The times are simulated.
32 devices in a mesh: fs: 16 (over z, y, core), tp: 2 (over x).
Axes of the slice: x: 2, y: 2, z: 4, core: 2. Of those that a mesh axis runs over, the one named last changes fastest.
Arguments:
- inputs: bfloat16 [16384, 3072], P('fs'), may hold values from -6 to 6
- query_cot: bfloat16 [16384, 768], P('fs', 'tp'), may hold values from -0.046875 to 0.046875
- value_cot: bfloat16 [16384, 1536], P('fs', 'tp'), may hold values from -0.046875 to 0.046875
- query_factor: bfloat16 [3072, 192], P('fs'), may hold values from -0.109375 to 0.109375
- value_factor: bfloat16 [3072, 192], P('fs'), may hold values from -0.109375 to 0.109375
- query_weight: float32 [3072, 768], P('fs', 'tp'), may hold values from -0.109375 to 0.109375
- value_weight: float32 [3072, 1536], P('fs', 'tp'), may hold values from -0.109375 to 0.109375
- query_first: float32 [192, 768], P('fs', 'tp'), may hold values from -1.6 to 1.6
- query_second: float32 [192, 768], P('fs', 'tp'), may hold values from 0.002 to 0.05
- value_first: float32 [192, 1536], P('fs', 'tp'), may hold values from -1.6 to 1.6
- value_second: float32 [192, 1536], P('fs', 'tp'), may hold values from 0.002 to 0.05
Outputs:
- step_q: float32 [3072, 768], P('fs', 'tp')
- step_v: float32 [3072, 1536], P('fs', 'tp')
- new_q: float32 [3072, 768], P('fs', 'tp')
- new_v: float32 [3072, 1536], P('fs', 'tp')
- first_q: float32 [192, 768], P('fs', 'tp')
- second_q: float32 [192, 768], P('fs', 'tp')
- first_v: float32 [192, 1536], P('fs', 'tp')
- second_v: float32 [192, 1536], P('fs', 'tp')
- copy_q: bfloat16 [3072, 768], P(None, 'tp')
- copy_v: bfloat16 [3072, 1536], P(None, 'tp')
All inputs are finite; a program needn't handle non-finite values.
Results may differ from a plain program's by a relative error of at most 0.0041.
Values may be sent and summed in bfloat16 or wider, within the bound.
A program may use at most 64 MiB of HBM per device.

v0:
```python
import functools

import jax
import jax.numpy as jnp
from jax import lax
from jax.experimental import pallas as pl
from jax.experimental.pallas import tpu as pltpu
from jax.sharding import PartitionSpec as P

first_decay = 0.9
second_decay = 0.99
small_eps = 1e-08
learn_rate = 0.01
CORES = 2
COLS = 2


def moments(old_first, old_second, gradient):
    first = first_decay * old_first + (1.0 - first_decay) * gradient
    second = second_decay * old_second + (1.0 - second_decay) * gradient * gradient
    unit = first / (jnp.sqrt(second) + small_eps)
    return (first, second, unit)


class Place:
    def __init__(self, n, t):
        self.n, self.t = n, t
        self.depth = n // (COLS * CORES)
        self.me = lax.axis_index("fs")
        self.tp = lax.axis_index("tp")
        self.c = self.me % CORES
        self.y = (self.me // CORES) % COLS
        self.z = self.me // (CORES * COLS)

    def at(self, z, y, c):
        return (z * COLS + y) * CORES + c

    def up(self, k):
        return (self.z + k) % self.depth

    def down(self, k):
        return (self.z + self.depth - k) % self.depth


class Gather:
    def __init__(self, place, own, full, sems):
        self.p, self.own, self.full = place, own, full
        self.zs, self.zr, self.ys, self.yr, self.cs, self.cr = sems
        self.sent = []

    def _copy(self, src, slot, ss, rs, to):
        return pltpu.make_async_remote_copy(
            src_ref=src, dst_ref=self.full.at[slot], send_sem=ss, recv_sem=rs,
            device_id={"fs": to}, device_id_type=pl.DeviceIdType.MESH)

    def _go(self, copy):
        copy.start()
        self.sent.append(copy)

    def piece(self, k):
        slot = self.p.at(self.p.down(k), self.p.y, self.p.c)
        return slot, (self.own if k == 0 else self.full.at[slot])

    def send_z(self, k):
        p = self.p
        self._go(self._copy(self.own, p.me, self.zs.at[k], self.zr.at[k], p.at(p.up(k), p.y, p.c)))

    def wait_z(self, k):
        slot = self.p.at(self.p.down(k), self.p.y, self.p.c)
        self._copy(self.full.at[slot], slot, self.zs.at[k], self.zr.at[k], self.p.me).wait_recv()

    def send_yc(self, k):
        p = self.p
        slot, src = self.piece(k)
        self._go(self._copy(src, slot, self.ys.at[k], self.yr.at[k], p.at(p.z, 1 - p.y, p.c)))
        self._go(self._copy(src, slot, self.cs.at[0, k], self.cr.at[0, k], p.at(p.z, p.y, 1 - p.c)))

    def pass_y(self, k):
        p = self.p
        slot = p.at(p.down(k), 1 - p.y, p.c)
        got = self.full.at[slot]
        self._copy(got, slot, self.ys.at[k], self.yr.at[k], p.me).wait_recv()
        self._go(self._copy(got, slot, self.cs.at[1, k], self.cr.at[1, k], p.at(p.z, p.y, 1 - p.c)))

    def wait_c(self):
        p = self.p
        for j in range(2):
            for k in range(p.depth):
                slot = p.at(p.down(k), p.y if j == 0 else 1 - p.y, 1 - p.c)
                self._copy(self.full.at[slot], slot, self.cs.at[j, k], self.cr.at[j, k], p.me).wait_recv()

    def drain(self):
        for copy in self.sent:
            copy.wait_send()


def gather_sems(depth):
    dma = pltpu.SemaphoreType.DMA
    return [dma((depth,)), dma((depth,)), dma((depth,)), dma((depth,)), dma((2, depth)), dma((2, depth))]


class Line:
    def __init__(self, place, own, full, sems):
        self.p, self.own, self.full = place, own, full
        self.zs, self.zr, self.ys, self.yr, self.cs, self.cr = sems
        self.sent = []

    def _copy(self, src, slot, ss, rs, to):
        return pltpu.make_async_remote_copy(
            src_ref=src, dst_ref=self.full.at[slot], send_sem=ss, recv_sem=rs,
            device_id={"fs": to}, device_id_type=pl.DeviceIdType.MESH)

    def _go(self, when, make):
        pl.when(when)(lambda: make().start())
        self.sent.append((when, make))

    def origin(self, d, s):
        z = self.p.z - 1 - s if d == 0 else self.p.z + 1 + s
        return z, (z >= 0 if d == 0 else z < self.p.depth)

    def send(self, s):
        p = self.p
        for d in range(2):
            to, frm = (p.z + 1, p.z - s) if d == 0 else (p.z - 1, p.z + s)
            when = jnp.logical_and(to < p.depth, frm >= 0) if d == 0 else jnp.logical_and(to >= 0, frm < p.depth)

            def make(d=d, to=to, frm=frm):
                slot = p.at(frm, p.y, p.c)
                src = self.own if s == 0 else self.full.at[slot]
                return self._copy(src, slot, self.zs.at[d, s], self.zr.at[d, s], p.at(to, p.y, p.c))

            self._go(when, make)

    def wait(self, s):
        p = self.p
        for d in range(2):
            z, when = self.origin(d, s)

            @pl.when(when)
            def _(d=d, z=z):
                slot = p.at(z, p.y, p.c)
                self._copy(self.full.at[slot], slot, self.zs.at[d, s], self.zr.at[d, s], p.me).wait_recv()

    def own_yc(self):
        p, k = self.p, self.p.depth - 1
        self._go(True, lambda: self._copy(
            self.own, p.me, self.ys.at[0, k], self.yr.at[0, k], p.at(p.z, 1 - p.y, p.c)))
        self._go(True, lambda: self._copy(
            self.own, p.me, self.cs.at[0, 0, k], self.cr.at[0, 0, k], p.at(p.z, p.y, 1 - p.c)))

    def forward(self, d, s, also=True):
        p = self.p
        z, when = self.origin(d, s)
        when = jnp.logical_and(when, also)

        def to_y():
            slot = p.at(z, p.y, p.c)
            return self._copy(self.full.at[slot], slot, self.ys.at[d, s], self.yr.at[d, s], p.at(p.z, 1 - p.y, p.c))

        def to_c():
            slot = p.at(z, p.y, p.c)
            return self._copy(
                self.full.at[slot], slot, self.cs.at[0, d, s], self.cr.at[0, d, s], p.at(p.z, p.y, 1 - p.c))

        self._go(when, to_y)
        self._go(when, to_c)

    def items(self):
        last = self.p.depth - 1
        yield 0, last, self.p.z, True
        for s in range(last):
            for d in range(2):
                z, when = self.origin(d, s)
                yield d, s, z, when

    def pass_y(self):
        p = self.p
        for d, s, z, when in self.items():
            slot = p.at(z, 1 - p.y, p.c)

            @pl.when(when)
            def _(d=d, s=s, slot=slot):
                got = self.full.at[slot]
                self._copy(got, slot, self.ys.at[d, s], self.yr.at[d, s], p.me).wait_recv()

            self._go(when, lambda d=d, s=s, slot=slot: self._copy(
                self.full.at[slot], slot, self.cs.at[1, d, s], self.cr.at[1, d, s], p.at(p.z, p.y, 1 - p.c)))

    def wait_c(self):
        p = self.p
        for j in range(2):
            for d, s, z, when in self.items():
                slot = p.at(z, p.y if j == 0 else 1 - p.y, 1 - p.c)

                @pl.when(when)
                def _(d=d, s=s, slot=slot):
                    self._copy(self.full.at[slot], slot, self.cs.at[j, d, s], self.cr.at[j, d, s], p.me).wait_recv()

    def drain(self):
        for when, make in self.sent:
            pl.when(when)(lambda make=make: make().wait_send())


def line_sems(depth):
    dma = pltpu.SemaphoreType.DMA
    return [dma((2, depth))] * 4 + [dma((2, 2, depth))] * 2


def kernel(
    n, t, x_hbm, cq_hbm, cv_hbm, qf_hbm, vf_hbm, qw_hbm, vw_hbm, q1_hbm, q2_hbm, v1_hbm, v2_hbm,
    w_all, f_all, bits, grad,
    x, cq, cv, qf, vf, qw, vw, q1, q2, v1, v2,
    f_own, w_own, g, gc_in, gs, gy_in, gt, gz_in, u_own, u_all, u_flat, sq, sq_in,
    acc_q, acc_v, local, gsem, tsem, *sems):
    p = Place(n, t)
    depth = p.depth
    rows = q1.shape[0]
    rank, q_cols = acc_q.shape
    v_cols = acc_v.shape[1]
    F = Gather(p, f_own, f_all, sems[0:6])
    W = Line(p, w_own, w_all, sems[6:12])
    U = Gather(p, u_own, u_all, sems[12:18])
    pairs = (
        (qf_hbm, qf), (vf_hbm, vf), (qw_hbm, qw), (vw_hbm, vw), (x_hbm, x), (cq_hbm, cq), (cv_hbm, cv),
        (q1_hbm, q1), (q2_hbm, q2), (v1_hbm, v1), (v2_hbm, v2))
    loads = [pltpu.make_async_copy(src, dst, local.at[i]) for i, (src, dst) in enumerate(pairs)]
    for copy in loads:
        copy.start()

    barrier = pltpu.get_barrier_semaphore()
    peers = [{"fs": p.at(p.up(k), p.y, p.c)} for k in range(1, depth)]
    peers += [{"fs": p.at(p.z, 1 - p.y, p.c)}, {"fs": p.at(p.z, p.y, 1 - p.c)}]
    peers += [{"tp": (p.tp + k) % t} for k in range(1, t)]
    for peer in peers:
        pl.semaphore_signal(barrier, inc=1, device_id=peer, device_id_type=pl.DeviceIdType.MESH)
    loads[0].wait()
    loads[1].wait()
    f_own[:, :rank] = qf[...]
    f_own[:, rank:] = vf[...]
    pl.semaphore_wait(barrier, len(peers))

    for k in range(1, depth):
        F.send_z(k)
    F.send_yc(0)
    f_all[p.me] = f_own[...]
    loads[2].wait()
    loads[3].wait()
    w_own[:, :q_cols] = qw[...].astype(jnp.bfloat16)
    w_own[:, q_cols:] = vw[...].astype(jnp.bfloat16)
    w_all[p.me] = w_own[...]
    for k in range(1, depth):
        F.wait_z(k)
        F.send_yc(k)
    W.own_yc()
    W.send(0)
    for k in range(depth):
        F.pass_y(k)
    F.wait_c()
    for copy in loads[4:]:
        copy.wait()

    acc_q[...] = jnp.zeros_like(acc_q)
    acc_v[...] = jnp.zeros_like(acc_v)
    tile = 256

    @pl.loop(0, x.shape[0] // tile)
    def _(i):
        at = pl.ds(pl.multiple_of(i * tile, tile), tile)
        f = f_all[...].reshape(x.shape[1], 2 * rank)
        proj = jnp.dot(x[at, :], f, preferred_element_type=jnp.float32)
        turned = proj.T.astype(jnp.bfloat16)
        acc_q[...] += jnp.dot(turned[:rank], cq[at, :], preferred_element_type=jnp.float32)
        acc_v[...] += jnp.dot(turned[rank:], cv[at, :], preferred_element_type=jnp.float32)

    for j in range(n):
        c, y, z = j % CORES, (j // CORES) % COLS, j // (CORES * COLS)
        g[c, y, z, :, :q_cols] = acc_q[j * rows:(j + 1) * rows, :]
        g[c, y, z, :, q_cols:] = acc_v[j * rows:(j + 1) * rows, :]

    def swap(src, dst, k, peer):
        return pltpu.make_async_remote_copy(
            src_ref=src, dst_ref=dst, send_sem=gsem.at[0, k], recv_sem=gsem.at[1, k],
            device_id=peer, device_id_type=pl.DeviceIdType.MESH)

    to_core = swap(g.at[1 - p.c], gc_in, 0, {"fs": p.at(p.z, p.y, 1 - p.c)})
    to_core.start()
    W.wait(0)
    W.send(1)
    to_core.wait()
    gs[...] = g[p.c] + gc_in[...]
    to_col = swap(gs.at[1 - p.y], gy_in, depth, {"fs": p.at(p.z, 1 - p.y, p.c)})
    to_col.start()
    W.forward(0, 0)
    W.forward(1, 0, p.z == 0)
    to_col.wait()
    gt[...] = gs[p.y] + gy_in[...]
    to_z = [swap(gt.at[p.up(k)], gz_in.at[k - 1], k, {"fs": p.at(p.up(k), p.y, p.c)}) for k in range(1, depth)]
    for copy in to_z:
        copy.start()
    total = gt[p.z]
    for k, copy in enumerate(to_z):
        copy.wait()
        total = total + gz_in[k]
    grad[...] = total
    u_own[:, :q_cols] = moments(q1[...], q2[...], total[:, :q_cols])[2]
    u_own[:, q_cols:] = moments(v1[...], v2[...], total[:, q_cols:])[2]
    for k in range(1, depth):
        U.send_z(k)
    U.send_yc(0)
    for s in range(1, depth - 2):
        W.wait(s)
        W.send(s + 1)
        if s == 1:
            u_all[p.me] = u_own[...]
            for k in range(1, depth):
                U.wait_z(k)
                U.send_yc(k)
            W.forward(1, 0, p.z > 0)
        for d in range(2):
            W.forward(d, s)
    for k in range(depth):
        U.pass_y(k)
    U.wait_c()
    for j in range(n):
        u_flat[j * rows:(j + 1) * rows, :] = u_all[j]
    own_sq = jnp.sum(u_flat[...] * u_flat[...])
    sq[...] = jnp.full(sq.shape, own_sq, jnp.float32)
    shares = [
        pltpu.make_async_remote_copy(
            src_ref=sq, dst_ref=sq_in.at[k - 1], send_sem=tsem.at[0, k], recv_sem=tsem.at[1, k],
            device_id={"tp": (p.tp + k) % t}, device_id_type=pl.DeviceIdType.MESH)
        for k in range(1, t)
    ]
    for copy in shares:
        copy.start()
    W.wait(depth - 2)
    for d in range(2):
        W.forward(d, depth - 2)
    norm = sq[...]
    for k, copy in enumerate(shares):
        copy.wait()
        norm = norm + sq_in[k]
    entries = rank * (q_cols + v_cols) * t
    scale = lax.rsqrt(norm[:1, :1] / entries + 1e-06)
    bits[...] = (scale * u_flat[...]).astype(jnp.bfloat16)
    W.pass_y()
    W.wait_c()
    F.drain()
    U.drain()
    W.drain()


def exchange(*args):
    inputs, query_cot, value_cot, query_factor, value_factor, query_weight, value_weight = args[:7]
    n, t = lax.axis_size("fs"), lax.axis_size("tp")
    depth = n // (COLS * CORES)
    rows, q_cols = args[7].shape
    v_cols = args[9].shape[1]
    cols = q_cols + v_cols
    rank, deep = rows * n, query_factor.shape[0]
    any_, vmem = pl.BlockSpec(memory_space=pl.ANY), pl.BlockSpec(memory_space=pltpu.VMEM)
    f32, bf16 = jnp.float32, jnp.bfloat16
    dma = pltpu.SemaphoreType.DMA
    shape = jax.ShapeDtypeStruct
    w_all, f_all, bits, grad = pl.pallas_call(
        functools.partial(kernel, n, t),
        out_shape=(
            shape((n, deep, cols), bf16), shape((n, deep, 2 * rank), bf16), shape((rank, cols), bf16),
            shape((rows, cols), f32),
        ),
        in_specs=[any_] * len(args),
        out_specs=(vmem,) * 4,
        scratch_shapes=[pltpu.VMEM(a.shape, a.dtype) for a in args] + [
            pltpu.VMEM((deep, 2 * rank), bf16), pltpu.VMEM((deep, cols), bf16),
            pltpu.VMEM((CORES, COLS, depth, rows, cols), f32), pltpu.VMEM((COLS, depth, rows, cols), f32),
            pltpu.VMEM((COLS, depth, rows, cols), f32), pltpu.VMEM((depth, rows, cols), f32),
            pltpu.VMEM((depth, rows, cols), f32), pltpu.VMEM((depth - 1, rows, cols), f32),
            pltpu.VMEM((rows, cols), f32), pltpu.VMEM((n, rows, cols), f32), pltpu.VMEM((rank, cols), f32),
            pltpu.VMEM((8, 128), f32), pltpu.VMEM((t - 1, 8, 128), f32),
            pltpu.VMEM((rank, q_cols), f32), pltpu.VMEM((rank, v_cols), f32),
            dma((len(args),)), dma((2, depth + 1)), dma((2, t)),
        ] + gather_sems(depth) + line_sems(depth) + gather_sems(depth),
        compiler_params=pltpu.CompilerParams(
            collective_id=0, has_side_effects=True, vmem_limit_bytes=54 * 1024 * 1024 - 65536),
    )(*args)
    first_q, second_q, _ = moments(args[7], args[8], grad[:, :q_cols])
    first_v, second_v, _ = moments(args[9], args[10], grad[:, q_cols:])
    return w_all, f_all, bits, first_q, second_q, first_v, second_v


def by_collectives(
    inputs, query_cot, value_cot, query_factor, value_factor, query_weight, value_weight,
    query_first, query_second, value_first, value_second,
):
    f_own = jnp.concatenate([query_factor, value_factor], axis=1)
    w_own = jnp.concatenate([query_weight, value_weight], axis=1).astype(jnp.bfloat16)
    q_cols = query_cot.shape[1]
    n, rank = lax.axis_size("fs"), f_own.shape[1] // 2
    entries = rank * (q_cols + value_cot.shape[1]) * lax.axis_size("tp")
    f_all = lax.all_gather(f_own, "fs", axis=0)
    w_all = lax.all_gather(w_own, "fs", axis=0)
    proj = jnp.dot(inputs, f_all.reshape(-1, 2 * rank), preferred_element_type=jnp.float32).astype(jnp.bfloat16)
    over = (((0,), (0,)), ((), ()))
    term_q = lax.dot_general(proj[:, :rank], query_cot, over, preferred_element_type=jnp.float32)
    term_v = lax.dot_general(proj[:, rank:], value_cot, over, preferred_element_type=jnp.float32)
    own = lax.psum_scatter(jnp.concatenate([term_q, term_v], axis=1), "fs", scatter_dimension=0, tiled=True)
    first_q, second_q, unit_q = moments(query_first, query_second, own[:, :q_cols])
    first_v, second_v, unit_v = moments(value_first, value_second, own[:, q_cols:])
    total = lax.psum(jnp.sum(unit_q * unit_q) + jnp.sum(unit_v * unit_v), ("fs", "tp"))
    scale = lax.rsqrt(total / entries + 1e-06)
    mine = (scale * jnp.concatenate([unit_q, unit_v], axis=1)).astype(jnp.bfloat16)
    bits = lax.all_gather(mine, "fs", axis=0, tiled=True)
    return w_all, f_all, bits, first_q, second_q, first_v, second_v


def copy_kernel(w, f, bits, copy_q, copy_v):
    rank, q_cols = f.shape[2] // 2, copy_q.shape[1]
    for i in range(w.shape[0]):
        deep = w.shape[1]
        at = slice(i * deep, (i + 1) * deep)
        step_q = jnp.dot(f[i][:, :rank], bits[:, :q_cols], preferred_element_type=jnp.float32)
        step_v = jnp.dot(f[i][:, rank:], bits[:, q_cols:], preferred_element_type=jnp.float32)
        copy_q[at, :] = (w[i][:, :q_cols].astype(jnp.float32) - learn_rate * step_q).astype(jnp.bfloat16)
        copy_v[at, :] = (w[i][:, q_cols:].astype(jnp.float32) - learn_rate * step_v).astype(jnp.bfloat16)


def copies(w_all, f_all, bits, q_cols):
    n, deep, cols = w_all.shape
    some = 2
    shape = jax.ShapeDtypeStruct
    return pl.pallas_call(
        copy_kernel,
        grid=(n // some,),
        out_shape=(shape((n * deep, q_cols), jnp.bfloat16), shape((n * deep, cols - q_cols), jnp.bfloat16)),
        in_specs=[
            pl.BlockSpec((some, deep, cols), lambda i: (i, 0, 0)),
            pl.BlockSpec((some,) + f_all.shape[1:], lambda i: (i, 0, 0)),
            pl.BlockSpec(bits.shape, lambda i: (0, 0)),
        ],
        out_specs=(
            pl.BlockSpec((some * deep, q_cols), lambda i: (i, 0)),
            pl.BlockSpec((some * deep, cols - q_cols), lambda i: (i, 0)),
        ),
    )(w_all, f_all, bits)


def on_device(
    inputs, query_cot, value_cot, query_factor, value_factor, query_weight, value_weight,
    query_first, query_second, value_first, value_second,
):
    n = lax.axis_size("fs")
    rank, q_cols, v_cols = query_factor.shape[1], query_cot.shape[1], value_cot.shape[1]
    whole = (
        n % (COLS * CORES) == 0 and n >= 4 * COLS * CORES and lax.axis_size("tp") > 1 and q_cols % 128 == 0
        and v_cols % 128 == 0 and (2 * rank) % 128 == 0 and inputs.shape[1] % 128 == 0
        and inputs.shape[0] % 256 == 0 and query_factor.shape[0] % 16 == 0 and rank % 16 == 0
    )
    run = exchange if whole else by_collectives
    w_all, f_all, bits, first_q, second_q, first_v, second_v = run(
        inputs, query_cot, value_cot, query_factor, value_factor, query_weight, value_weight,
        query_first, query_second, value_first, value_second)
    if whole:
        step_q = jnp.dot(query_factor, bits[:, :q_cols], preferred_element_type=jnp.float32)
        step_v = jnp.dot(value_factor, bits[:, q_cols:], preferred_element_type=jnp.float32)
        new_q = query_weight - learn_rate * step_q
        new_v = value_weight - learn_rate * step_v
        copy_q, copy_v = copies(w_all, f_all, bits, q_cols)
        return (step_q, step_v, new_q, new_v, first_q, second_q, first_v, second_v, copy_q, copy_v)
    f_full = f_all.reshape(-1, 2 * rank)
    w_full = w_all.reshape(-1, q_cols + v_cols)
    bits_q, bits_v = bits[:, :q_cols], bits[:, q_cols:]
    f32 = jnp.float32
    step_q = jnp.dot(query_factor, bits_q, preferred_element_type=f32)
    step_v = jnp.dot(value_factor, bits_v, preferred_element_type=f32)
    new_q = query_weight - learn_rate * step_q
    new_v = value_weight - learn_rate * step_v
    all_q = jnp.dot(f_full[:, :rank], bits_q, preferred_element_type=f32)
    all_v = jnp.dot(f_full[:, rank:], bits_v, preferred_element_type=f32)
    copy_q = (w_full[:, :q_cols].astype(f32) - learn_rate * all_q).astype(jnp.bfloat16)
    copy_v = (w_full[:, q_cols:].astype(f32) - learn_rate * all_v).astype(jnp.bfloat16)
    return (step_q, step_v, new_q, new_v, first_q, second_q, first_v, second_v, copy_q, copy_v)


def solution(mesh):
    row, both = P("fs", None), P("fs", "tp")
    in_specs = (row, both, both, row, row) + (both,) * 6
    out_specs = (both,) * 8 + (P(None, "tp"),) * 2
    return jax.shard_map(on_device, mesh=mesh, in_specs=in_specs, out_specs=out_specs, check_vma=False)
```

profile of v0, /device:TPU:0, one launch (start us, length us, event | category | flops | bytes accessed | tf_op | source)
XLA Modules:
  0.0 102.3 jit_solution(11880445770452402021)
XLA Ops:
  0.6 87.7 %shard_map.186 = (bf16[16,192,1152]{2,1,0:T(8,128)(2,1)}, bf16[16,192,384]{2,1,0:T(8,128)(2,1)}, bf16[192,1152]{1,0:T(8,128)(2,1)}, f32[12,1152]{1,0:T(8,128)}) custom-call(bf16[1024,3072]{1,0:T(8,128)(2,1)} %x_hbm.1, bf16[1024,384]{1,0:T(8,128)(2,1)} %cq_hbm.1, bf16[1024,768]{1,0:T(8,128)(2,1)} %cv_hbm.1, bf16[192,192]{1,0:T(8,128)(2,1)} %qf_hbm.1, ...), custom_call_target="tpu_custom_call" | custom-call | tf_op jit(solution)/shard_map/pallas_call | solution.py:365
  88.3 0.0 copy-start.7
  88.4 0.0 copy-start.8
  88.4 0.0 copy-start.9
  88.4 0.0 copy-start.5
  88.4 0.0 copy-start.6
  88.4 0.0 copy-start.1
  88.4 0.0 copy-start.2
  88.4 0.0 copy-start.4
  88.4 0.0 copy-start
  88.5 0.0 copy-start.3
  88.5 10.3 %shard_map.187 = (bf16[3072,384]{1,0:T(8,128)(2,1)}, bf16[3072,768]{1,0:T(8,128)(2,1)}) custom-call(bf16[16,192,1152]{2,1,0:T(8,128)(2,1)} %get-tuple-element.18.w, bf16[16,192,384]{2,1,0:T(8,128)(2,1)} %get-tuple-element.19.f, bf16[192,1152]{1,0:T(8,128)(2,1)} %get-tuple-element.16.bits), custom_call_target="tpu_custom_call" | custom-call | tf_op jit(solution)/shard_map/pallas_call | solution.py:431
  98.7 0.0 copy-done.7
  98.8 0.0 copy-done.8
  98.8 0.0 copy-done.9
  98.8 0.6 fusion.3
  99.4 0.0 copy-done.5
  99.4 0.0 copy-done.6
  99.4 0.7 fusion.2
  100.1 0.0 copy-done.1
  100.1 0.0 copy-done.2
  100.1 0.0 copy-done.4
  100.1 1.0 multiply_subtract_fusion.1
  101.1 0.0 copy-done
  101.1 0.0 copy-done.3
  101.1 1.2 %multiply_subtract_fusion = (f32[192,768]{1,0:T(8,128)}, f32[192,768]{1,0:T(8,128)}) fusion(f32[192,768]{1,0:T(8,128)S(1)} %copy-done, bf16[192,192]{1,0:T(8,128)(2,1)S(1)} %copy-done.3, bf16[192,1152]{1,0:T(8,128)(2,1)S(1)} %copy-done.1), kind=kOutput, calls=%fused_computation.2 | convolution fusion | flops 56918016 | bytes 2162688 | tf_op jit(solution)/shard_map/dot_general | solution.py:464
Async XLA Ops:
  88.3 10.4 %copy-start.7 = (f32[12,384]{1,0:T(8,128)S(1)}, f32[12,384]{1,0:T(8,128)}, u32[]{:S(2)}) copy-start(f32[12,384]{1,0:T(8,128)} %q1_hbm.1) | copy-start | bytes 55300
  88.4 10.4 %copy-start.8 = (f32[12,384]{1,0:T(8,128)S(1)}, f32[12,384]{1,0:T(8,128)}, u32[]{:S(2)}) copy-start(f32[12,384]{1,0:T(8,128)} %q2_hbm.1) | copy-start | bytes 55300
  88.4 10.4 %copy-start.9 = (f32[12,1152]{1,0:T(8,128)S(1)}, f32[12,1152]{1,0:T(8,128)}, u32[]{:S(2)}) copy-start(f32[12,1152]{1,0:T(8,128)} %get-tuple-element.17) | copy-start | bytes 165892
  88.4 11.0 %copy-start.5 = (f32[12,768]{1,0:T(8,128)S(1)}, f32[12,768]{1,0:T(8,128)}, u32[]{:S(2)}) copy-start(f32[12,768]{1,0:T(8,128)} %v1_hbm.1) | copy-start | bytes 110596
  88.4 11.0 %copy-start.6 = (f32[12,768]{1,0:T(8,128)S(1)}, f32[12,768]{1,0:T(8,128)}, u32[]{:S(2)}) copy-start(f32[12,768]{1,0:T(8,128)} %v2_hbm.1) | copy-start | bytes 110596
  88.4 11.6 %copy-start.1 = (bf16[192,1152]{1,0:T(8,128)(2,1)S(1)}, bf16[192,1152]{1,0:T(8,128)(2,1)}, u32[]{:S(2)}) copy-start(bf16[192,1152]{1,0:T(8,128)(2,1)} %get-tuple-element.16.bits) | copy-start | bytes 1327108
  88.4 11.6 %copy-start.2 = (f32[192,384]{1,0:T(8,128)S(1)}, f32[192,384]{1,0:T(8,128)}, u32[]{:S(2)}) copy-start(f32[192,384]{1,0:T(8,128)} %qw_hbm.1) | copy-start | bytes 884740
  88.4 11.6 %copy-start.4 = (bf16[192,192]{1,0:T(8,128)(2,1)S(1)}, bf16[192,192]{1,0:T(8,128)(2,1)}, u32[]{:S(2)}) copy-start(bf16[192,192]{1,0:T(8,128)(2,1)} %qf_hbm.1) | copy-start | bytes 221188
  88.4 12.6 %copy-start = (f32[192,768]{1,0:T(8,128)S(1)}, f32[192,768]{1,0:T(8,128)}, u32[]{:S(2)}) copy-start(f32[192,768]{1,0:T(8,128)} %vw_hbm.1) | copy-start | bytes 1769476
  88.5 12.6 %copy-start.3 = (bf16[192,192]{1,0:T(8,128)(2,1)S(1)}, bf16[192,192]{1,0:T(8,128)(2,1)}, u32[]{:S(2)}) copy-start(bf16[192,192]{1,0:T(8,128)(2,1)} %vf_hbm.1) | copy-start | bytes 221188
where the time goes:
time: 103 us; the launch traced here: 102 us
  Pallas kernels  98 us (95%)
  matrix products  2.25 us (2%)
  other arithmetic  1.28 us (1%)
    pallas_call x1, Pallas kernels, exchange(): pl.pallas_call(functools.partial(kernel, n, t), out_shape=(shape((n, deep...  87.7 us
    pallas_call x1, Pallas kernels, copies(): pl.pallas_call(copy_kernel, grid=(n // some,), out_shape=(shape((n * deep...  10.3 us

commit v1 on v0

v1 whole, which is shorter than its diff:
```python
import functools

import jax
import jax.numpy as jnp
from jax import lax
from jax.experimental import pallas as pl
from jax.experimental.pallas import tpu as pltpu
from jax.sharding import PartitionSpec as P

first_decay = 0.9
second_decay = 0.99
small_eps = 1e-08
learn_rate = 0.01
CORES = 2
COLS = 2
TPS = 2
HALVES = 2
DEPTH = 4
WIRE = jnp.bfloat16


def moments(old_first, old_second, gradient):
    first = first_decay * old_first + (1.0 - first_decay) * gradient
    second = second_decay * old_second + (1.0 - second_decay) * gradient * gradient
    unit = first / (jnp.sqrt(second) + small_eps)
    return (first, second, unit)


class Place:
    def __init__(self, n):
        self.depth = n // (COLS * CORES)
        self.me = lax.axis_index("fs")
        self.tp = lax.axis_index("tp")
        self.c = self.me % CORES
        self.y = (self.me // CORES) % COLS
        self.z = self.me // (CORES * COLS)

    def at(self, z, y, c):
        return (z * COLS + y) * CORES + c

    def near(self, i):
        if i == 0:
            return self.z
        below, above = self.z, self.depth - 1 - self.z
        both = jnp.minimum(below, above)
        turn = self.z - (i + 1) // 2 if i % 2 else self.z + i // 2
        far = jnp.where(below < above, self.z + (i - both), self.z - (i - both))
        return jnp.where(i <= 2 * both, turn, far)

    def col(self, j):
        return self.y if j == 0 else 1 - self.y

    def to_z(self, z):
        return {"fs": self.at(z, self.y, self.c)}

    def to_y(self):
        return {"fs": self.at(self.z, 1 - self.y, self.c)}

    def to_c(self):
        return {"fs": self.at(self.z, self.y, 1 - self.c)}

    def to_x(self):
        return {"tp": 1 - self.tp}


class Mail:
    def __init__(self, place):
        self.p = place
        self.sent = []

    def send(self, src, dst, ss, rs, peer, when=None):
        def make():
            return pltpu.make_async_remote_copy(
                src_ref=src, dst_ref=dst, send_sem=ss, recv_sem=rs,
                device_id=peer, device_id_type=pl.DeviceIdType.MESH)

        if when is None:
            make().start()
        else:
            pl.when(when)(lambda: make().start())
        self.sent.append((when, make))

    def got(self, dst, ss, rs):
        pltpu.make_async_remote_copy(
            src_ref=dst, dst_ref=dst, send_sem=ss, recv_sem=rs,
            device_id=self.p.to_c(), device_id_type=pl.DeviceIdType.MESH).wait_recv()

    def drain(self):
        for when, make in self.sent:
            if when is None:
                make().wait_send()
            else:
                pl.when(when)(lambda make=make: make().wait_send())


class Factors:
    def __init__(self, place, mail, full, spread, sems):
        self.p, self.m, self.full = place, mail, full
        self.zs, self.zr, self.ys, self.yr, self.xs, self.xr, self.cs, self.cr = sems
        rows = full.shape[1]
        rest = rows - spread
        self.mine = pl.ds(pl.multiple_of(place.tp * rest, 16), spread)
        self.give = pl.ds(pl.multiple_of(place.tp * spread, 16), rest)
        self.take = pl.ds(pl.multiple_of((1 - place.tp) * spread, 16), rest)

    def view(self, j, i, rows, c=None):
        p = self.p
        return self.full.at[p.at(p.near(i), p.col(j), p.c if c is None else c), rows]

    def own(self):
        p, v = self.p, self.view(0, 0, self.mine)
        for i in range(1, p.depth):
            self.m.send(v, v, self.zs.at[i], self.zr.at[p.z], p.to_z(p.near(i)))
        self.m.send(v, v, self.ys.at[0], self.yr.at[p.z], p.to_y())
        whole = self.full.at[p.me]
        self.m.send(whole, whole, self.cs.at[0, 0, 0], self.cr.at[0, 0, p.z], p.to_c())

    def pass_xc(self, j, i):
        p = self.p
        z = p.near(i)
        v, g = self.view(j, i, self.mine), self.view(j, i, self.give)
        self.m.send(g, g, self.xs.at[j, i], self.xr.at[j, z], p.to_x())
        self.m.send(v, v, self.cs.at[0, j, i], self.cr.at[0, j, z], p.to_c())

    def z(self, i):
        p = self.p
        v = self.view(0, i, self.mine)
        self.m.got(v, self.zs.at[i], self.zr.at[p.near(i)])
        self.m.send(v, v, self.ys.at[i], self.yr.at[p.near(i)], p.to_y())
        self.pass_xc(0, i)

    def y(self, i):
        v = self.view(1, i, self.mine)
        self.m.got(v, self.ys.at[i], self.yr.at[self.p.near(i)])
        self.pass_xc(1, i)

    def x(self, j, i):
        p = self.p
        z = p.near(i)
        v = self.view(j, i, self.take)
        self.m.got(v, self.xs.at[j, i], self.xr.at[j, z])
        self.m.send(v, v, self.cs.at[1, j, i], self.cr.at[1, j, z], p.to_c())

    def core(self, j, i):
        p = self.p
        z = p.near(i)
        if j == 0 and i == 0:
            self.m.got(self.full.at[p.at(z, p.y, 1 - p.c)], self.cs.at[0, 0, 0], self.cr.at[0, 0, z])
            return
        self.m.got(self.view(j, i, self.mine, 1 - p.c), self.cs.at[0, j, i], self.cr.at[0, j, z])
        self.m.got(self.view(j, i, self.take, 1 - p.c), self.cs.at[1, j, i], self.cr.at[1, j, z])


class Weights:
    def __init__(self, place, mail, full, sems):
        self.p, self.m, self.full = place, mail, full
        self.zs, self.es, self.zr, self.ys, self.yr, self.cs, self.cr = sems
        self.half = full.shape[1] // HALVES

    def view(self, j, i, h, c=None):
        p = self.p
        slot = p.at(p.near(i), p.col(j), p.c if c is None else c)
        return self.full.at[slot, pl.ds(h * self.half, self.half)]

    def own_z(self, h):
        p, v = self.p, self.view(0, 0, h)
        for d, to in ((0, p.z + 1), (1, p.z - 1)):
            ok = to < p.depth if d == 0 else to >= 0
            self.m.send(v, v, self.zs.at[d, 0, h], self.zr.at[p.z, h], p.to_z(to), ok)

    def to_core(self, j, i, h):
        p, v = self.p, self.view(j, i, h)
        self.m.send(v, v, self.cs.at[j, i, h], self.cr.at[j, p.near(i), h], p.to_c())

    def own_y(self, h):
        p, v = self.p, self.view(0, 0, h)
        self.m.send(v, v, self.ys.at[0, h], self.yr.at[p.z, h], p.to_y())

    def z(self, i, h):
        p, v = self.p, self.view(0, i, h)
        frm = p.near(i)
        self.m.got(v, self.zs.at[0, i, h], self.zr.at[frm, h])
        to = jnp.where(frm < p.z, p.z + 1, p.z - 1)
        ok = jnp.logical_and(to >= 0, to < p.depth)
        self.m.send(v, v, self.zs.at[0, i, h], self.zr.at[frm, h], p.to_z(to), ok)
        if h > 0 or i > 2:
            when = None
        else:
            when = jnp.logical_and(frm != p.z + 1, frm != p.z - 1)
        if not (h == 0 and i == 1):
            self.m.send(v, v, self.ys.at[i, h], self.yr.at[frm, h], p.to_y(), when)
        self.to_core(0, i, h)

    def y(self, i, h):
        p, v = self.p, self.view(1, i, h)
        self.m.got(v, self.ys.at[i, h], self.yr.at[p.near(i), h])
        if i == 0 and h == 0:
            for d, to in ((0, p.z + 1), (1, p.z - 1)):
                ok = to < p.depth if d == 0 else to >= 0
                self.m.send(v, v, self.es.at[d], self.yr.at[p.z, h], p.to_z(to), ok)
        self.to_core(1, i, h)

    def core(self, j, i):
        p = self.p
        for h in range(HALVES):
            self.m.got(self.view(j, i, h, 1 - p.c), self.cs.at[j, i, h], self.cr.at[j, p.near(i), h])


class Units:
    def __init__(self, place, mail, full, sems):
        self.p, self.m, self.full = place, mail, full
        self.zs, self.zr, self.ys, self.yr, self.cs, self.cr = sems

    def view(self, j, i, c=None):
        p = self.p
        return self.full.at[p.at(p.near(i), p.col(j), p.c if c is None else c)]

    def to_core(self, j, i):
        p, v = self.p, self.view(j, i)
        self.m.send(v, v, self.cs.at[j, i], self.cr.at[j, p.near(i)], p.to_c())

    def to_col(self, i):
        p, v = self.p, self.view(0, i)
        self.m.send(v, v, self.ys.at[i], self.yr.at[p.near(i)], p.to_y())

    def own(self):
        p, v = self.p, self.view(0, 0)
        for i in range(p.depth - 1, 0, -1):
            self.m.send(v, v, self.zs.at[i], self.zr.at[p.z], p.to_z(p.near(i)))
        self.to_col(0)
        self.to_core(0, 0)

    def z(self, i):
        self.m.got(self.view(0, i), self.zs.at[i], self.zr.at[self.p.near(i)])
        self.to_col(i)
        self.to_core(0, i)

    def y(self, i):
        self.m.got(self.view(1, i), self.ys.at[i], self.yr.at[self.p.near(i)])
        self.to_core(1, i)

    def core(self, j, i):
        p = self.p
        self.m.got(self.view(j, i, 1 - p.c), self.cs.at[j, i], self.cr.at[j, p.near(i)])


def semaphores(depth):
    dma = pltpu.SemaphoreType.DMA
    line = [dma((depth,))]
    factors = line * 4 + [dma((COLS, depth))] * 2 + [dma((2, COLS, depth))] * 2
    weights = [
        dma((2, depth, HALVES)), dma((2,)), dma((depth, HALVES)), dma((depth, HALVES)), dma((depth, HALVES)),
        dma((COLS, depth, HALVES)), dma((COLS, depth, HALVES))]
    units = line * 4 + [dma((COLS, depth))] * 2
    return factors, weights, units


def kernel(
    n, counts, x_hbm, cq_hbm, cv_hbm, qf_hbm, vf_hbm, qw_hbm, vw_hbm, q1_hbm, q2_hbm, v1_hbm, v2_hbm,
    step_q, step_v, new_q, new_v, first_q, second_q, first_v, second_v, copy_q, copy_v,
    x, cq, cv, qf, vf, qw, vw, q1, q2, v1, v2,
    f_all, w_all, u_all, g, g_core, g_send, g_col, g_line, g_deep, g_part, u_flat, u_half, sq, sq_in,
    acc_q, acc_v, local, gcs, gzs, gzr, tsem, *sems):
    p = Place(n)
    depth = p.depth
    rows = q1.shape[0]
    rank, q_cols = acc_q.shape
    deep = w_all.shape[1]
    m = Mail(p)
    n_f, n_w, _ = counts
    F = Factors(p, m, f_all, deep // 2, sems[:n_f])
    W = Weights(p, m, w_all, sems[n_f:n_f + n_w])
    U = Units(p, m, u_all, sems[n_f + n_w:])
    others = range(1, depth)
    pairs = (
        (qf_hbm, qf), (vf_hbm, vf), (qw_hbm, qw), (vw_hbm, vw), (x_hbm, x), (cq_hbm, cq), (cv_hbm, cv),
        (q1_hbm, q1), (q2_hbm, q2), (v1_hbm, v1), (v2_hbm, v2))
    loads = [pltpu.make_async_copy(src, dst, local.at[i]) for i, (src, dst) in enumerate(pairs)]
    for copy in loads:
        copy.start()

    scope = jax.named_scope
    barrier = pltpu.get_barrier_semaphore()
    peers = [p.to_z(p.near(i)) for i in others] + [p.to_y(), p.to_c(), p.to_x()]
    with scope("enter"):
        for peer in peers:
            pl.semaphore_signal(barrier, inc=1, device_id=peer, device_id_type=pl.DeviceIdType.MESH)
        loads[0].wait()
        loads[1].wait()
        f_all[p.me, :, :rank] = qf[...]
        f_all[p.me, :, rank:] = vf[...]
    with scope("barrier"):
        pl.semaphore_wait(barrier, len(peers))
    F.own()
    with scope("load_w"):
        loads[2].wait()
        loads[3].wait()
        w_all[p.me, :, :q_cols] = qw[...].astype(jnp.bfloat16)
        w_all[p.me, :, q_cols:] = vw[...].astype(jnp.bfloat16)
    for h in range(HALVES):
        W.own_z(h)
    for i in others:
        with scope(f"fz{i}"):
            F.z(i)
    for h in range(HALVES):
        W.own_y(h)
        W.to_core(0, 0, h)
    for i in range(depth):
        with scope(f"fy{i}"):
            F.y(i)
    for i in others:
        with scope(f"fx0{i}"):
            F.x(0, i)
    for i in range(depth):
        with scope(f"fx1{i}"):
            F.x(1, i)
    with scope("fc"):
        for j in range(COLS):
            for i in range(depth):
                F.core(j, i)
    with scope("wz10"):
        W.z(1, 0)
    with scope("wz20"):
        W.z(2, 0)
    with scope("wy00"):
        W.y(0, 0)
    with scope("loads"):
        for copy in loads[4:]:
            copy.wait()

    tile = 256
    with scope("mm"):
        acc_q[...] = jnp.zeros_like(acc_q)
        acc_v[...] = jnp.zeros_like(acc_v)

        @pl.loop(0, x.shape[0] // tile)
        def _(k):
            at = pl.ds(pl.multiple_of(k * tile, tile), tile)
            f = f_all[...].reshape(x.shape[1], 2 * rank)
            proj = jnp.dot(x[at, :], f, preferred_element_type=jnp.float32)
            turned = proj.T.astype(jnp.bfloat16)
            acc_q[...] += jnp.dot(turned[:rank], cq[at, :], preferred_element_type=jnp.float32)
            acc_v[...] += jnp.dot(turned[rank:], cv[at, :], preferred_element_type=jnp.float32)

    with scope("gstore"):
        for j in range(n):
            c, y, z = j % CORES, (j // CORES) % COLS, j // (CORES * COLS)
            at = slice(z * rows, (z + 1) * rows)
            g[c, y, at, :q_cols] = acc_q[j * rows:(j + 1) * rows, :]
            g[c, y, at, q_cols:] = acc_v[j * rows:(j + 1) * rows, :]

    other = g.at[1 - p.c]
    m.send(other, g_core, gcs.at[0], gcs.at[1], p.to_c())
    with scope("wz11"):
        W.z(1, 1)
    with scope("wz21"):
        W.z(2, 1)
    with scope("wy01"):
        W.y(0, 1)
    with scope("gcore"):
        m.got(g_core, gcs.at[0], gcs.at[1])
        g_send[...] = (g[p.c, 1 - p.y] + g_core[1 - p.y]).astype(g_send.dtype)
    m.send(g_send, g_col, gcs.at[2], gcs.at[3], p.to_y())
    with scope("wy10"):
        W.y(1, 0)
    with scope("wz30"):
        W.z(3, 0)
    with scope("gcol"):
        m.got(g_col, gcs.at[2], gcs.at[3])
        mine = g[p.c, p.y] + g_core[p.y] + g_col[...].astype(jnp.float32)
        for z in range(depth):
            part = mine[z * rows:(z + 1) * rows]
            g_part[z] = part
            g_line[z] = part.astype(g_line.dtype)
    for i in range(depth - 1, 0, -1):
        to = p.near(i)
        m.send(g_line.at[to], g_deep.at[p.z], gzs.at[i], gzr.at[p.z], p.to_z(to))
    with scope("wy11"):
        W.y(1, 1)
    with scope("gline"):
        total = g_part[p.z]
        for i in others:
            frm = p.near(i)
            m.got(g_deep.at[frm], gzs.at[i], gzr.at[frm])
            total = total + g_deep[frm].astype(jnp.float32)
    with scope("moments"):
        first, second, unit = moments(q1[...], q2[...], total[:, :q_cols])
        first_q[...], second_q[...] = first, second
        u_all[p.me, :, :q_cols] = unit.astype(u_all.dtype)
        first, second, unit = moments(v1[...], v2[...], total[:, q_cols:])
        first_v[...], second_v[...] = first, second
        u_all[p.me, :, q_cols:] = unit.astype(u_all.dtype)
    U.own()
    for i in others:
        with scope(f"uz{i}"):
            U.z(i)
    for i in range(depth):
        with scope(f"uy{i}"):
            U.y(i)
    with scope("uc"):
        for j in range(COLS):
            for i in range(depth):
                U.core(j, i)
    with scope("norm"):
        for j in range(n):
            u_flat[j * rows:(j + 1) * rows, :] = u_all[j].astype(jnp.float32)
        whole = u_flat[...]
        u_half[...] = whole.astype(jnp.bfloat16)
        sq[...] = jnp.full(sq.shape, jnp.sum(whole * whole), jnp.float32)
        m.send(sq, sq_in, tsem.at[0], tsem.at[1], p.to_x())
    with scope("wz31"):
        W.z(3, 1)
    for i in range(2, depth):
        for h in range(HALVES):
            with scope(f"wy{i}{h}"):
                W.y(i, h)
    with scope("sq"):
        m.got(sq_in, tsem.at[0], tsem.at[1])
        entries = rank * (q_cols + acc_v.shape[1]) * TPS
        scale = lax.rsqrt((sq[:1, :1] + sq_in[:1, :1]) / entries + 1e-06)
        rate = learn_rate * scale

    def products(slot):
        f = f_all[slot]
        return (jnp.dot(f[:, :rank], u_half[:, :q_cols], preferred_element_type=jnp.float32),
                jnp.dot(f[:, rank:], u_half[:, q_cols:], preferred_element_type=jnp.float32))

    def renew(slot, got_q, got_v):
        at = pl.ds(pl.multiple_of(slot * deep, 16), deep)
        copy_q[at, :] = (w_all[slot, :, :q_cols].astype(jnp.float32) - rate * got_q).astype(jnp.bfloat16)
        copy_v[at, :] = (w_all[slot, :, q_cols:].astype(jnp.float32) - rate * got_v).astype(jnp.bfloat16)

    with scope("own"):
        got_q, got_v = products(p.me)
        renew(p.me, got_q, got_v)
        step_q[...] = scale * got_q
        step_v[...] = scale * got_v
        new_q[...] = qw[...] - rate * got_q
        new_v[...] = vw[...] - rate * got_v
    for i in range(depth):
        for j in range(COLS):
            if i + j > 0:
                with scope(f"mine{j}{i}"):
                    slot = p.at(p.near(i), p.col(j), p.c)
                    renew(slot, *products(slot))
    for i in range(depth):
        for j in range(COLS):
            with scope(f"wc{j}{i}"):
                W.core(j, i)
            with scope(f"theirs{j}{i}"):
                slot = p.at(p.near(i), p.col(j), 1 - p.c)
                renew(slot, *products(slot))
    with scope("drain"):
        m.drain()


def exchange(*args):
    n = lax.axis_size("fs")
    depth = n // (COLS * CORES)
    rows, q_cols = args[7].shape
    v_cols = args[9].shape[1]
    cols = q_cols + v_cols
    rank, deep = rows * n, args[3].shape[0]
    any_, vmem = pl.BlockSpec(memory_space=pl.ANY), pl.BlockSpec(memory_space=pltpu.VMEM)
    f32, bf16 = jnp.float32, jnp.bfloat16
    dma = pltpu.SemaphoreType.DMA
    part = rank // (CORES * COLS)
    groups = semaphores(depth)
    out = pltpu.VMEM
    done = pl.pallas_call(
        functools.partial(kernel, n, tuple(len(group) for group in groups)),
        out_shape=(
            out((deep, q_cols), f32), out((deep, v_cols), f32), out((deep, q_cols), f32), out((deep, v_cols), f32),
            out((rows, q_cols), f32), out((rows, q_cols), f32), out((rows, v_cols), f32), out((rows, v_cols), f32),
            out((n * deep, q_cols), bf16), out((n * deep, v_cols), bf16),
        ),
        in_specs=[any_] * len(args),
        out_specs=(vmem,) * 10,
        scratch_shapes=[pltpu.VMEM(a.shape, a.dtype) for a in args] + [
            pltpu.VMEM((n, deep, 2 * rank), bf16), pltpu.VMEM((n, deep, cols), bf16), pltpu.VMEM((n, rows, cols), bf16),
            pltpu.VMEM((CORES, COLS, part, cols), f32), pltpu.VMEM((COLS, part, cols), f32),
            pltpu.VMEM((part, cols), WIRE), pltpu.VMEM((part, cols), WIRE), pltpu.VMEM((depth, rows, cols), WIRE),
            pltpu.VMEM((depth, rows, cols), WIRE), pltpu.VMEM((depth, rows, cols), f32),
            pltpu.VMEM((rank, cols), f32), pltpu.VMEM((rank, cols), bf16),
            pltpu.VMEM((8, 128), f32), pltpu.VMEM((8, 128), f32),
            pltpu.VMEM((rank, q_cols), f32), pltpu.VMEM((rank, v_cols), f32),
            dma((len(args),)), dma((4,)), dma((depth,)), dma((depth,)), dma((2,)),
        ] + sum(groups, []),
        compiler_params=pltpu.CompilerParams(
            collective_id=0, has_side_effects=True, vmem_limit_bytes=50 * 1024 * 1024),
    )(*args)
    return write_out(done)


def write_kernel(*refs):
    sems, count = refs[-1], len(refs) // 2
    copies = [
        pltpu.make_async_copy(src, dst, sems.at[i]) for i, (src, dst) in enumerate(zip(refs[:count], refs[count:-1]))]
    for copy in copies:
        copy.start()
    for copy in copies:
        copy.wait()


def write_out(arrays):
    count = len(arrays)
    any_ = pl.BlockSpec(memory_space=pl.ANY)
    arrays = [pltpu.with_memory_space_constraint(a, pltpu.VMEM) for a in arrays]
    return pl.pallas_call(
        write_kernel,
        out_shape=tuple(pltpu.HBM(a.shape, a.dtype) for a in arrays),
        in_specs=[any_] * count,
        out_specs=(any_,) * count,
        scratch_shapes=[pltpu.SemaphoreType.DMA((count,))],
        compiler_params=pltpu.CompilerParams(has_side_effects=True, vmem_limit_bytes=1024 * 1024),
    )(*arrays)


def by_collectives(
    inputs, query_cot, value_cot, query_factor, value_factor, query_weight, value_weight,
    query_first, query_second, value_first, value_second,
):
    f_own = jnp.concatenate([query_factor, value_factor], axis=1)
    w_own = jnp.concatenate([query_weight, value_weight], axis=1).astype(jnp.bfloat16)
    q_cols = query_cot.shape[1]
    n, rank = lax.axis_size("fs"), f_own.shape[1] // 2
    entries = rank * (q_cols + value_cot.shape[1]) * lax.axis_size("tp")
    f_all = lax.all_gather(f_own, "fs", axis=0)
    w_all = lax.all_gather(w_own, "fs", axis=0)
    proj = jnp.dot(inputs, f_all.reshape(-1, 2 * rank), preferred_element_type=jnp.float32).astype(jnp.bfloat16)
    over = (((0,), (0,)), ((), ()))
    term_q = lax.dot_general(proj[:, :rank], query_cot, over, preferred_element_type=jnp.float32)
    term_v = lax.dot_general(proj[:, rank:], value_cot, over, preferred_element_type=jnp.float32)
    own = lax.psum_scatter(jnp.concatenate([term_q, term_v], axis=1), "fs", scatter_dimension=0, tiled=True)
    first_q, second_q, unit_q = moments(query_first, query_second, own[:, :q_cols])
    first_v, second_v, unit_v = moments(value_first, value_second, own[:, q_cols:])
    total = lax.psum(jnp.sum(unit_q * unit_q) + jnp.sum(unit_v * unit_v), ("fs", "tp"))
    scale = lax.rsqrt(total / entries + 1e-06)
    mine = (scale * jnp.concatenate([unit_q, unit_v], axis=1)).astype(jnp.bfloat16)
    bits = lax.all_gather(mine, "fs", axis=0, tiled=True)
    f_full = f_all.reshape(-1, 2 * rank)
    w_full = w_all.reshape(-1, w_own.shape[1])
    bits_q, bits_v = bits[:, :q_cols], bits[:, q_cols:]
    f32 = jnp.float32
    step_q = jnp.dot(query_factor, bits_q, preferred_element_type=f32)
    step_v = jnp.dot(value_factor, bits_v, preferred_element_type=f32)
    new_q = query_weight - learn_rate * step_q
    new_v = value_weight - learn_rate * step_v
    all_q = jnp.dot(f_full[:, :rank], bits_q, preferred_element_type=f32)
    all_v = jnp.dot(f_full[:, rank:], bits_v, preferred_element_type=f32)
    copy_q = (w_full[:, :q_cols].astype(f32) - learn_rate * all_q).astype(jnp.bfloat16)
    copy_v = (w_full[:, q_cols:].astype(f32) - learn_rate * all_v).astype(jnp.bfloat16)
    return (step_q, step_v, new_q, new_v, first_q, second_q, first_v, second_v, copy_q, copy_v)


def on_device(*args):
    n = lax.axis_size("fs")
    inputs, query_cot, value_cot, query_factor = args[:4]
    rank, q_cols, v_cols = query_factor.shape[1], query_cot.shape[1], value_cot.shape[1]
    whole = (
        n == DEPTH * COLS * CORES and lax.axis_size("tp") == TPS and q_cols % 128 == 0
        and v_cols % 128 == 0 and (2 * rank) % 128 == 0 and inputs.shape[1] % 128 == 0
        and inputs.shape[0] % 256 == 0 and query_factor.shape[0] % 32 == 0 and rank % 64 == 0
    )
    return (exchange if whole else by_collectives)(*args)


def solution(mesh):
    row, both = P("fs", None), P("fs", "tp")
    in_specs = (row, both, both, row, row) + (both,) * 6
    out_specs = (both,) * 8 + (P(None, "tp"),) * 2
    return jax.shard_map(on_device, mesh=mesh, in_specs=in_specs, out_specs=out_specs, check_vma=False)
```

time: 103 us -> 86 us (0.83)
  Pallas kernels: 98 us -> 85.2 us
  matrix products: 2.25 us -> 0 us
  other arithmetic: 1.28 us -> 0 us
    pallas_call x2, Pallas kernels: 98 us -> 85.2 us  [the longest x1 81.5 us: exchange(): pl.pallas_call(functools.partial(kernel, n, tuple((len(group) for group i...]
    dot_general x2 -> x0, matrix products: 2.25 us -> none  [the longest x1 1.24 us: on_device(): jnp.dot(value_factor, bits[:, q_cols:], preferred_element_type=jnp.float32)]
    add x2 -> x0, other arithmetic: 1.28 us -> none  [moments(): second_decay * old_second + (1.0 - second_decay) * gradient * gradient]
where the time goes in v1:
time: 86 us; the launch traced here: 85.8 us
  Pallas kernels  85.2 us (99%)
    pallas_call x1, Pallas kernels, exchange(): pl.pallas_call(functools.partial(kernel, n, tuple((len(group) for group i...  81.5 us
    pallas_call x1, Pallas kernels, write_out(): pl.pallas_call(write_kernel, out_shape=tuple((pltpu.HBM(a.shape, a.dtype)...  3.69 us

profile of v1, /device:TPU:0, one launch (start us, length us, event | category | flops | bytes accessed | tf_op | source)
XLA Modules:
  0.0 85.8 jit_solution(16428063609642492918)
XLA Ops:
  0.6 81.5 %shard_map.186 = (f32[192,384]{1,0:T(8,128)S(1)}, f32[192,768]{1,0:T(8,128)S(1)}, f32[192,384]{1,0:T(8,128)S(1)}, f32[192,768]{1,0:T(8,128)S(1)}, f32[12,384]{1,...) custom-call(bf16[1024,3072]{1,0:T(8,128)(2,1)} %x_hbm.1, ...), custom_call_target="tpu_custom_call" | custom-call | tf_op jit(solution)/shard_map/pallas_call | solution.py:470
  82.1 3.7 %shard_map.187 = (f32[192,384]{1,0:T(8,128)}, f32[192,768]{1,0:T(8,128)}, f32[192,384]{1,0:T(8,128)}, f32[192,768]{1,0:T(8,128)}, f32[12,384]{1,0:T(8,128)}, /*i...) custom-call(f32[192,384]{1,0:T(8,128)S(1)} %get-tuple-element.20.ref, ...), custom_call_target="tpu_custom_call" | custom-call | tf_op jit(solution)/shard_map/pallas_call | solution.py:509
